TPU v7x, 32 devices: a whole 2x2x4 slice. The times are simulated.
32 devices in a mesh: dp: 4 (over y, x), kv: 4 (over z), tp: 2 (over core).
Axes of the slice: x: 2, y: 2, z: 4, core: 2. Of those that a mesh axis runs over, the one named last changes fastest.
Arguments:
- tokens: bfloat16 [16, 4096], P('dp', ('kv', 'tp')), may hold values from -24 to 24
- rec_state: float32 [16, 16, 128, 128], P(('dp', 'kv'), 'tp'), may hold values from -2 to 2
- norm_gain: float32 [4096], replicated, may hold values from 0.1 to 1.9
- w_query: bfloat16 [4096, 2048], P('kv', 'tp'), may hold values from -0.09375 to 0.09375
- w_forget: bfloat16 [4096, 2048], P('kv', 'tp'), may hold values from -0.09375 to 0.09375
- w_input: bfloat16 [4096, 2048], P('kv', 'tp'), may hold values from -0.09375 to 0.09375
- w_outgate: bfloat16 [4096, 2048], P('kv', 'tp'), may hold values from -0.09375 to 0.09375
- lower_bound: float32 [2048], P('tp'), may hold values from 0 to 0.9
- head_gain: float32 [2048], P('tp'), may hold values from 0.1 to 1.9
- w_heads_out: bfloat16 [2048, 4096], P(None, ('kv', 'tp')), may hold values from -0.125 to 0.125
- mixer_gain: float32 [4096], replicated, may hold values from 0.1 to 1.9
- w_gate: bfloat16 [4096, 11264], P(None, ('kv', 'tp')), may hold values from -0.09375 to 0.09375
- w_up: bfloat16 [4096, 11264], P(None, ('kv', 'tp')), may hold values from -0.09375 to 0.09375
- w_down: bfloat16 [11264, 4096], P(('kv', 'tp')), may hold values from -0.078125 to 0.078125
Outputs:
- result: bfloat16 [16, 4096], P('dp', ('kv', 'tp'))
- new_state: float32 [16, 16, 128, 128], P(('dp', 'kv'), 'tp')
All inputs are finite; a program needn't handle non-finite values.
Results may differ from a plain program's by a relative error of at most 0.012.
Values may be sent and summed in bfloat16 or wider, within the bound.
A program may use at most 128 MiB of HBM per device.

v0:
```python
import jax
import jax.numpy as jnp
from jax import lax
from jax.sharding import PartitionSpec as P

HEAD_DIM = 128


epsilon = 1e-06


def channel_mixer(whole_rows, mixer_gain, w_gate, w_up, w_down):
    rows_float = whole_rows.astype(jnp.float32)
    mixer_scale = lax.rsqrt(jnp.mean(rows_float * rows_float, axis=1, keepdims=True) + epsilon)
    normed = (rows_float * mixer_scale * mixer_gain).astype(jnp.bfloat16)
    gate_val = jnp.dot(normed, w_gate, preferred_element_type=jnp.float32)
    up_val = jnp.dot(normed, w_up, preferred_element_type=jnp.float32)
    hidden = (jax.nn.silu(gate_val) * up_val).astype(jnp.bfloat16)
    return jnp.dot(hidden, w_down, preferred_element_type=jnp.float32)


def local(
    tokens,
    rec_state,
    norm_gain,
    w_query,
    w_forget,
    w_input,
    w_outgate,
    lower_bound,
    head_gain,
    w_heads_out,
    mixer_gain,
    w_gate,
    w_up,
    w_down,
):
    kv_count = lax.axis_size("kv")
    tp_count = lax.axis_size("tp")
    kv_index = lax.axis_index("kv")
    row_count = tokens.shape[0]
    seq_count = rec_state.shape[0]
    model_width = norm_gain.shape[0]
    col_block = model_width // kv_count
    tok_float = tokens.astype(jnp.float32)
    whole_rows = lax.all_gather(tokens, ("kv", "tp"), axis=1, tiled=True).astype(jnp.float32)
    squares = jnp.sum(whole_rows * whole_rows, axis=1)
    own_cols = lax.dynamic_slice_in_dim(whole_rows, kv_index * col_block, col_block, 1)
    gain_block = lax.dynamic_slice_in_dim(norm_gain, kv_index * col_block, col_block, 0)
    scaled = (own_cols * gain_block).astype(jnp.bfloat16)
    projected = lax.psum_scatter(
        jnp.stack(
            [
                jnp.dot(scaled, weight, preferred_element_type=jnp.float32)
                for weight in (w_query, w_forget, w_input, w_outgate)
            ],
            axis=1,
        ),
        "kv",
        scatter_dimension=0,
        tiled=True,
    )
    my_squares = lax.dynamic_slice_in_dim(squares, kv_index * seq_count, seq_count, 0)
    row_scale = lax.rsqrt(my_squares / model_width + epsilon)[:, None]
    query_pre = row_scale * projected[:, 0]
    forget_pre = row_scale * projected[:, 1]
    value_in = row_scale * projected[:, 2]
    gate_pre = row_scale * projected[:, 3]
    forget = lower_bound + (1.0 - lower_bound) * jax.nn.sigmoid(forget_pre)
    key_in = 1.0 - forget
    query_act = jax.nn.silu(query_pre)
    head_count = rec_state.shape[1]
    shaped = (seq_count, head_count, HEAD_DIM)
    forget = forget.reshape(shaped)
    key_in = key_in.reshape(shaped)
    value_in = value_in.reshape(shaped)
    query_act = query_act.reshape(shaped)
    new_state = forget[:, :, :, None] * rec_state + key_in[:, :, :, None] * value_in[:, :, None, :]
    head_out = jnp.sum(query_act[:, :, :, None] * new_state, axis=2)
    head_out = head_out * lax.rsqrt(jnp.mean(head_out * head_out, axis=2, keepdims=True) + epsilon)
    head_out = head_out * head_gain.reshape(head_count, HEAD_DIM)
    local_width = head_count * HEAD_DIM
    gated = (head_out.reshape(seq_count, local_width) * jax.nn.silu(gate_pre)).astype(jnp.bfloat16)
    every_head = lax.all_gather(gated[None], ("kv", "tp"), axis=0, tiled=True)
    every_head = every_head.reshape(kv_count, tp_count, seq_count, local_width)
    every_head = every_head.transpose(0, 2, 1, 3).reshape(
        kv_count * seq_count, tp_count * local_width
    )
    mixed_add = jnp.dot(every_head, w_heads_out, preferred_element_type=jnp.float32)
    mixed = (tok_float + mixed_add).astype(jnp.bfloat16)
    gathered = lax.all_gather(mixed, ("kv", "tp"), axis=1, tiled=True)
    terms = channel_mixer(gathered, mixer_gain, w_gate, w_up, w_down)
    out_block = model_width // (kv_count * tp_count)
    blocked = terms.reshape(row_count, kv_count, tp_count, out_block)
    chip_sum = lax.psum_scatter(blocked.astype(jnp.bfloat16), "tp", scatter_dimension=2, tiled=True)
    down_sum = (
        lax.psum_scatter(chip_sum, "kv", scatter_dimension=1, tiled=True)
        .astype(jnp.float32)
        .reshape(row_count, out_block)
    )
    result = (mixed.astype(jnp.float32) + down_sum).astype(jnp.bfloat16)
    return (result, new_state)


def solution(mesh):
    placed = (
        P("dp", ("kv", "tp")),
        P(("dp", "kv"), "tp", None, None),
        P(),
        P("kv", "tp"),
        P("kv", "tp"),
        P("kv", "tp"),
        P("kv", "tp"),
        P("tp"),
        P("tp"),
        P(None, ("kv", "tp")),
        P(),
        P(None, ("kv", "tp")),
        P(None, ("kv", "tp")),
        P(("kv", "tp"), None),
    )
    return jax.shard_map(
        local,
        mesh=mesh,
        in_specs=placed,
        out_specs=(P("dp", ("kv", "tp")), P(("dp", "kv"), "tp", None, None)),
        check_vma=False,
    )
```

profile of v0, /device:TPU:0, one launch (start us, length us, event | category | flops | bytes accessed | tf_op | source)
XLA Modules:
  0.0 140.6 jit_solution(1454577620565583170)
XLA Ops:
  7.2 0.0 copy-start
  7.2 0.0 all-reduce.5.cloned.1.call-start
  7.2 16.1 %all_gather.9 = bf16[4,4096]{1,0:T(4,128)(2,1)S(1)} all-gather(bf16[4,512]{1,0:T(4,128)(2,1)} %param.14), channel_id=1, replica_groups=mesh['dp'=4,'kv'=4,'tp'=2] {'kv','tp'}, dimensions={1}, use_global_device_ids=true | all-gather | bytes 36864 | tf_op jit(solution)/shard_map/all_gather | solution.py:46
  23.3 0.8 dynamic_slice.11
  24.2 0.4 convolution_bitcast_fusion
  24.6 0.3 copy-done.1
  24.9 0.4 convolution_bitcast_fusion.1
  25.3 0.6 copy-done.2
  25.9 0.4 convolution_bitcast_fusion.2
  26.3 0.3 copy-done.3
  26.7 0.4 convolution_bitcast_fusion.3
  27.1 0.7 copy.18
  27.7 0.0 all-reduce.5.cloned.1.call-update
  27.8 0.6 dynamic-slice.2
  28.4 0.6 dynamic-slice
  29.0 0.1 multiply_reduce_fusion.1
  29.1 0.6 dynamic_slice.9
  30.4 32.8 %all-reduce.5.cloned.1.call-done = f32[4,4,1024]{2,1,0:T(4,128)} async-done(((f32[4,4,1024]{2,1,0:T(4,128)}), f32[4,4,1024]{2,1,0:T(4,128)}) %all-reduce.5.cloned.1.call-update) | async-done | bytes 65552
  63.2 1.5 %dynamic-slice_multiply_fusion = (f32[1,1,1024]{2,1,0:T(1,128)S(1)}, f32[1,1,1024]{2,1,0:T(1,128)S(1)}, f32[1,1,1024]{2,1,0:T(1,128)S(1)}, f32[1,1,1024]{2,1,0:T(1,128)S(1)}) fusion(f32[4,4,1024]{2,1,0:T(4,128)} %all-reduce.5.cloned.1.call-done, u32[]{:T(128)} %bitcast.19, u32[]{:T(128)S(6)} %convert.4, f32[]{:T(128)} %bitcast, u32[]{:T(128)S(6)} %convert.3, ...), kind=kLoop, calls=%fused_computation.26 | loop fusion | flops 7168 | bytes 32788 | tf_op jit(solution)/shard_map/mul | solution.py:68
  64.8 1.3 multiply_reduce_fusion
  66.0 0.1 multiply_reduce_fusion.2
  66.1 0.1 mul.206
  66.2 12.8 %all-gather = bf16[8192]{0:T(1024)(128)(2,1)S(1)} all-gather(bf16[1024]{0:T(1024)(128)(2,1)S(1)} %fusion.13), channel_id=2, replica_groups=mesh['dp'=4,'kv'=4,'tp'=2] {'kv','tp'}, dimensions={0}, use_global_device_ids=true | all-gather | bytes 18432 | tf_op jit(solution)/shard_map/all_gather | solution.py:84
  79.0 2.0 %fusion.1 = bf16[4,512]{1,0:T(4,128)(2,1)S(1)} fusion(bf16[4,2048]{1,0:T(4,128)(2,1)S(1)} %reshape_transpose_reshape.3, bf16[2048,512]{1,0:T(8,128)(2,1)} %param.23, bf16[4,512]{1,0:T(4,128)(2,1)S(1)} %copy-done.6), kind=kOutput, calls=%fused_computation.8 | convolution fusion | flops 8394752 | bytes 2121728 | tf_op jit(solution)/shard_map/dot_general | solution.py:89
  81.0 14.1 %all_gather.11 = bf16[4,4096]{1,0:T(4,128)(2,1)S(1)} all-gather(bf16[4,512]{1,0:T(4,128)(2,1)S(1)} %fusion.1), channel_id=1, replica_groups=mesh['dp'=4,'kv'=4,'tp'=2] {'kv','tp'}, dimensions={1}, use_global_device_ids=true | all-gather | bytes 36864 | tf_op jit(solution)/shard_map/all_gather | solution.py:91
  95.1 0.1 fusion.2
  95.2 5.9 %fusion.18 = f32[4,1408]{1,0:T(4,128)S(1)} fusion(bf16[4096,1408]{1,0:T(8,128)(2,1)} %param.25, bf16[4,4096]{1,0:T(4,128)(2,1)S(1)} %all_gather.11, f32[4096]{0:T(1024)S(1)} %copy-done.5, f32[4]{0:T(128)S(1)} %add_rsqrt_fusion), kind=kOutput, calls=%fused_computation.45 | convolution fusion | flops 46202880 | bytes 11606032 | tf_op jit(solution)/shard_map/dot_general | solution.py:16
  101.1 11.0 %convolution_convert_fusion = bf16[4,4096]{1,0:T(4,128)(2,1)S(1)} fusion(bf16[1408,4096]{1,0:T(8,128)(2,1)} %param.27, bf16[4096,1408]{1,0:T(8,128)(2,1)} %param.26, f32[4,1408]{1,0:T(4,128)S(1)} %fusion.18, bf16[4,4096]{1,0:T(4,128)(2,1)S(1)} %all_gather.11, f32[4096]{0:T(1024)S(1)} %copy-done.5, f32[4]{0:T(128)S(1)} %add_rsqrt_fusion), kind=kOutput, calls=%fused_computation | convolution fusion | flops 92390400 | bytes 23173136 | tf_op jit(solution)/shard_map/dot_general | solution.py:19
  112.1 3.6 %all-reduce.1 = bf16[4,4,2,512]{3,0,2,1:T(4,128)(2,1)S(1)} all-reduce(bf16[4,4,2,512]{3,0,2,1:T(4,128)(2,1)S(1)} %bitcast.49), channel_id=4, replica_groups=mesh['dp'=4,'kv'=4,'tp'=2] {'tp'}, use_global_device_ids=true, to_apply=%region_5.6.clone | all-reduce | flops 16384 | bytes 65536
  115.7 0.6 constant_dynamic-slice_fusion
  116.4 16.2 %all-reduce.2 = bf16[4,4,1,512]{3,0,2,1:T(4,128)(2,1)S(1)} all-reduce(bf16[4,4,1,512]{3,0,2,1:T(4,128)(2,1)S(1)} %constant_dynamic-slice_fusion), channel_id=5, replica_groups=mesh['dp'=4,'kv'=4,'tp'=2] {'kv'}, use_global_device_ids=true, to_apply=%region_6.7.clone | all-reduce | flops 8192 | bytes 32768
  132.6 1.2 fusion.9
  (27 shorter events, 0.1 us)
Async XLA Ops:
  7.2 17.0 %copy-start = (bf16[1024,1024]{1,0:T(8,128)(2,1)S(1)}, bf16[1024,1024]{1,0:T(8,128)(2,1)}, u32[]{:S(2)}) copy-start(bf16[1024,1024]{1,0:T(8,128)(2,1)} %param.20) | copy-start | bytes 6291460
  7.2 56.0 %all-reduce.5.cloned.1.call-start = ((), (), s32[]{:S(2)}) async-start(), calls=%async_computation | async-start | bytes 131072
  23.3 1.6 %copy-start.1 = (bf16[1024,1024]{1,0:T(8,128)(2,1)S(1)}, bf16[1024,1024]{1,0:T(8,128)(2,1)}, u32[]{:S(2)}) copy-start(bf16[1024,1024]{1,0:T(8,128)(2,1)} %param.19) | copy-start | bytes 6291460
  24.2 1.8 %copy-start.2 = (bf16[1024,1024]{1,0:T(8,128)(2,1)S(1)}, bf16[1024,1024]{1,0:T(8,128)(2,1)}, u32[]{:S(2)}) copy-start(bf16[1024,1024]{1,0:T(8,128)(2,1)} %param.18) | copy-start | bytes 6291460
  24.9 1.7 %copy-start.3 = (bf16[1024,1024]{1,0:T(8,128)(2,1)S(1)}, bf16[1024,1024]{1,0:T(8,128)(2,1)}, u32[]{:S(2)}) copy-start(bf16[1024,1024]{1,0:T(8,128)(2,1)} %param.17) | copy-start | bytes 6291460
  25.9 1.8 %copy-start.10 = (u32[32]{0:T(128)S(1)}, u32[32]{0:T(128)}, u32[]{:S(2)}) copy-start(u32[32]{0:T(128)} %constant.45) | copy-start | bytes 388
  25.9 2.4 %copy-start.9 = (u32[32]{0:T(128)S(1)}, u32[32]{0:T(128)}, u32[]{:S(2)}) copy-start(u32[32]{0:T(128)} %constant.41) | copy-start | bytes 388
  25.9 38.8 %copy-start.7 = (f32[1024]{0:T(1024)S(1)}, f32[1024]{0:T(1024)}, u32[]{:S(2)}) copy-start(f32[1024]{0:T(1024)} %param.21) | copy-start | bytes 12292
  25.9 38.8 %copy-start.4 = (f32[1,8,128,128]{3,2,1,0:T(8,128)S(1)}, f32[1,8,128,128]{3,2,1,0:T(8,128)}, u32[]{:S(2)}) copy-start(f32[1,8,128,128]{3,2,1,0:T(8,128)} %param.15) | copy-start | bytes 1572868
  26.6 39.6 %copy-start.8 = (f32[1024]{0:T(1024)S(1)}, f32[1024]{0:T(1024)}, u32[]{:S(2)}) copy-start(f32[1024]{0:T(1024)} %param.22) | copy-start | bytes 12292
  26.7 52.4 %copy-start.6 = (bf16[4,512]{1,0:T(4,128)(2,1)S(1)}, bf16[4,512]{1,0:T(4,128)(2,1)}, u32[]{:S(2)}) copy-start(bf16[4,512]{1,0:T(4,128)(2,1)} %param.14) | copy-start | bytes 12292
  27.0 68.2 %copy-start.5 = (f32[4096]{0:T(1024)S(1)}, f32[4096]{0:T(1024)}, u32[]{:S(2)}) copy-start(f32[4096]{0:T(1024)} %param.24) | copy-start | bytes 49156
Sparse Core Ops, SparseCore 0:
  27.9 35.2 all-reduce.4
where the time goes:
time: 141 us
  blocking collectives  62.7 us (44%)
  waiting for transfers between devices  32.8 us (23%)
  matrix products  20.4 us (14%)
  between operations  14.9 us (11%)
  local copies, waits for them, and re-layouts  5.37 us (4%)
  other arithmetic  4.46 us (3%)
    unnamed x2, waiting for transfers between devices  32.8 us
    unnamed x2, blocking collectives  19.8 us
    all_gather x1, blocking collectives, local(): lax.all_gather(tokens, ('kv', 'tp'), axis=1, tiled=True).astype(jnp.float32)  16.1 us
    all_gather x1, blocking collectives, local(): gathered = lax.all_gather(mixed, ('kv', 'tp'), axis=1, tiled=True)  14.1 us
    all_gather x1, blocking collectives, local(): every_head = lax.all_gather(gated[None], ('kv', 'tp'), axis=0, tiled=True)  12.8 us
    dot_general x1, matrix products, channel_mixer(): return jnp.dot(hidden, w_down, preferred_element_type=jnp.float32)  11 us
    dot_general x1, matrix products, channel_mixer(): gate_val = jnp.dot(normed, w_gate, preferred_element_type=jnp.float32)  5.9 us
    unnamed x25, local copies, waits for them, and re-layouts  3.18 us
  transfers between devices with their start and end apart: 1, of which 1 were waited for; matrix products, arithmetic and copies ran while one was open for 1% of the time, Pallas kernels for 0%

commit v1 on v0

--- a/solution.py
+++ b/solution.py
@@ -1,6 +1,10 @@
+import functools
+
 import jax
 import jax.numpy as jnp
 from jax import lax
+from jax.experimental import pallas as pl
+from jax.experimental.pallas import tpu as pltpu
 from jax.sharding import PartitionSpec as P
 
 HEAD_DIM = 128
@@ -19,7 +23,7 @@
     return jnp.dot(hidden, w_down, preferred_element_type=jnp.float32)
 
 
-def local(
+def local_plain(
     tokens,
     rec_state,
     norm_gain,
@@ -102,6 +106,435 @@
     return (result, new_state)
 
 
+LANES = 128
+MESH = pl.DeviceIdType.MESH
+
+
+def silu(v):
+    return v / (1.0 + jnp.exp(-v))
+
+
+def layer_kernel(
+    kv_count,
+    tp_count,
+    tokens,
+    rec_state,
+    norm_gain,
+    w_query,
+    w_forget,
+    w_input,
+    w_outgate,
+    lower_bound,
+    head_gain,
+    w_heads_out,
+    mixer_gain,
+    w_gate,
+    w_up,
+    w_down,
+    result,
+    new_state,
+    tok_all,
+    state_in,
+    state_out,
+    ngain_buf,
+    lower_buf,
+    hgain_buf,
+    mgain_buf,
+    proj_w,
+    heads_w,
+    gate_w,
+    up_w,
+    down_w,
+    proj_send,
+    proj_recv,
+    head_rows,
+    gated_all,
+    gated_float,
+    mixed_all,
+    gate_acc,
+    up_acc,
+    hidden_buf,
+    down_send,
+    down_recv,
+    small_sem,
+    proj_sem,
+    heads_sem,
+    gate_sem,
+    up_sem,
+    down_sem,
+    tok_ssem,
+    tok_rsem,
+    proj_ssem,
+    proj_rsem,
+    gated_ssem,
+    gated_rsem,
+    mixed_ssem,
+    mixed_rsem,
+    red_ssem,
+    red_rsem,
+):
+    kv = lax.axis_index("kv")
+    tp = lax.axis_index("tp")
+    group = kv_count * tp_count
+    me = kv * tp_count + tp
+    rows, cols = tokens.shape
+    head_count = rec_state.shape[1]
+    width = cols * group
+    proj_rows = cols * tp_count
+
+    def coords(index):
+        return {"kv": lax.div(index, tp_count), "tp": lax.rem(index, tp_count)}
+
+    def ahead(step):
+        return lax.rem(me + step, group)
+
+    def behind(step):
+        return lax.rem(me + group - step, group)
+
+    def rows_of(step):
+        return pl.ds(pl.multiple_of(behind(step) * cols, LANES), cols)
+
+    def cols_of(step):
+        return pl.ds(pl.multiple_of(ahead(step) * cols, LANES), cols)
+
+    tok_copy = pltpu.make_async_copy(tokens, tok_all.at[tp], small_sem.at[0])
+    small_copies = [
+        pltpu.make_async_copy(norm_gain, ngain_buf, small_sem.at[1]),
+        pltpu.make_async_copy(lower_bound, lower_buf, small_sem.at[2]),
+        pltpu.make_async_copy(head_gain, hgain_buf, small_sem.at[3]),
+        pltpu.make_async_copy(mixer_gain, mgain_buf, small_sem.at[4]),
+    ]
+    state_copy = pltpu.make_async_copy(rec_state.at[0], state_in, small_sem.at[5])
+    proj_copies = [
+        pltpu.make_async_copy(weight, proj_w.at[i], proj_sem.at[i])
+        for i, weight in enumerate((w_query, w_forget, w_input, w_outgate))
+    ]
+    heads_copy = pltpu.make_async_copy(w_heads_out, heads_w, heads_sem)
+
+    def gate_copy(step):
+        return pltpu.make_async_copy(w_gate.at[rows_of(step), :], gate_w.at[step], gate_sem.at[step])
+
+    def up_copy(step):
+        return pltpu.make_async_copy(w_up.at[rows_of(step), :], up_w.at[step], up_sem.at[step])
+
+    def down_copy(step):
+        return pltpu.make_async_copy(w_down.at[:, cols_of(step)], down_w.at[step], down_sem.at[step])
+
+    tok_copy.start()
+    for copy in small_copies:
+        copy.start()
+    for copy in proj_copies:
+        copy.start()
+    state_copy.start()
+    heads_copy.start()
+
+    barrier = pltpu.get_barrier_semaphore()
+    for step in range(1, group):
+        pl.semaphore_signal(barrier, inc=1, device_id=coords(ahead(step)), device_id_type=MESH)
+    for step in range(group):
+        gate_copy(step).start()
+        up_copy(step).start()
+    for step in range(group):
+        down_copy(step).start()
+    pl.semaphore_wait(barrier, group - 1)
+
+    tok_copy.wait()
+    tok_sends = []
+    for step in range(1, tp_count):
+        send = pltpu.make_async_remote_copy(
+            src_ref=tok_all.at[tp],
+            dst_ref=tok_all.at[tp],
+            send_sem=tok_ssem.at[step],
+            recv_sem=tok_rsem.at[step],
+            device_id={"tp": lax.rem(tp + step, tp_count)},
+            device_id_type=MESH,
+        )
+        send.start()
+        tok_sends.append(send)
+    for copy in small_copies:
+        copy.wait()
+    for step in range(1, tp_count):
+        source = lax.rem(tp + tp_count - step, tp_count)
+        pltpu.make_async_remote_copy(
+            src_ref=tok_all.at[source],
+            dst_ref=tok_all.at[source],
+            send_sem=tok_ssem.at[step],
+            recv_sem=tok_rsem.at[step],
+            device_id={"tp": source},
+            device_id_type=MESH,
+        ).wait_recv()
+
+    tok_float = jnp.concatenate([tok_all[i].astype(jnp.float32) for i in range(tp_count)], axis=1)
+    squares = jnp.sum(tok_float * tok_float, axis=1, keepdims=True)
+    per_block = proj_rows // LANES
+    gain_row = jnp.concatenate(
+        [ngain_buf[pl.ds(kv * per_block + i, 1), :] for i in range(per_block)], axis=1
+    )
+    scaled = (tok_float * gain_row).astype(jnp.bfloat16)
+    square_rows = jnp.broadcast_to(squares, (rows, LANES))
+    for h in range(head_count):
+        proj_send[:, 4, h, :] = square_rows
+
+    @pl.loop(0, 4)
+    def _(which):
+        pltpu.make_async_copy(w_query, proj_w.at[which], proj_sem.at[which]).wait()
+        part = jnp.dot(scaled, proj_w[which], preferred_element_type=jnp.float32)
+        for h in range(head_count):
+            proj_send[:, which, h, :] = part[:, h * LANES : (h + 1) * LANES]
+
+    proj_sends = []
+    for step in range(1, kv_count):
+        target = lax.rem(kv + step, kv_count)
+        send = pltpu.make_async_remote_copy(
+            src_ref=proj_send.at[target],
+            dst_ref=proj_recv.at[step],
+            send_sem=proj_ssem.at[step],
+            recv_sem=proj_rsem.at[step],
+            device_id={"kv": target},
+            device_id_type=MESH,
+        )
+        send.start()
+        proj_sends.append(send)
+    total = proj_send[kv]
+    state_copy.wait()
+    for step in range(1, kv_count):
+        proj_sends[step - 1].wait_recv()
+        total = total + proj_recv[step]
+    row_scale = lax.rsqrt(total[4] / width + epsilon)
+    query_act = silu(row_scale * total[0])
+    lower = lower_buf[...]
+    forget = lower + (1.0 - lower) / (1.0 + jnp.exp(-(row_scale * total[1])))
+    key_in = 1.0 - forget
+    value_in = row_scale * total[2]
+    gate_act = silu(row_scale * total[3])
+    forget_t = forget.T
+    key_t = key_in.T
+    query_t = query_act.T
+    for h in range(head_count):
+        fresh = forget_t[:, h : h + 1] * state_in[h] + key_t[:, h : h + 1] * value_in[h : h + 1, :]
+        state_out[h] = fresh
+        head_rows[h : h + 1, :] = jnp.sum(query_t[:, h : h + 1] * fresh, axis=0, keepdims=True)
+    head_out = head_rows[...]
+    head_out = head_out * lax.rsqrt(jnp.mean(head_out * head_out, axis=1, keepdims=True) + epsilon)
+    gated_all[0] = (head_out * hgain_buf[...] * gate_act).astype(jnp.bfloat16)
+
+    gated_sends = []
+    for step in range(1, group):
+        send = pltpu.make_async_remote_copy(
+            src_ref=gated_all.at[0],
+            dst_ref=gated_all.at[step],
+            send_sem=gated_ssem.at[step],
+            recv_sem=gated_rsem.at[step],
+            device_id=coords(ahead(step)),
+            device_id_type=MESH,
+        )
+        send.start()
+        gated_sends.append(send)
+    state_store = pltpu.make_async_copy(state_out, new_state.at[0], small_sem.at[6])
+    state_store.start()
+    gated_float[kv, tp] = gated_all[0].astype(jnp.float32)
+    heads_copy.wait()
+    for step in range(1, group):
+        gated_sends[step - 1].wait_recv()
+        source = behind(step)
+        gated_float[lax.div(source, tp_count), lax.rem(source, tp_count)] = gated_all[step].astype(jnp.float32)
+    every_head = jnp.concatenate(
+        [gated_float[:, t, h, :] for t in range(tp_count) for h in range(head_count)], axis=1
+    ).astype(jnp.bfloat16)
+    mixed_add = jnp.dot(every_head, heads_w[...], preferred_element_type=jnp.float32)
+    mixed = (tok_all[tp].astype(jnp.float32) + mixed_add).astype(jnp.bfloat16)
+    mixed_all[0] = mixed
+
+    mixed_sends = []
+    for step in range(1, group):
+        send = pltpu.make_async_remote_copy(
+            src_ref=mixed_all.at[0],
+            dst_ref=mixed_all.at[step],
+            send_sem=mixed_ssem.at[step],
+            recv_sem=mixed_rsem.at[step],
+            device_id=coords(ahead(step)),
+            device_id_type=MESH,
+        )
+        send.start()
+        mixed_sends.append(send)
+
+    gate_acc[...] = jnp.zeros_like(gate_acc)
+    up_acc[...] = jnp.zeros_like(up_acc)
+    per_cols = cols // LANES
+
+    def mixer_step(step, squares_sum):
+        mixed_float = mixed_all[step].astype(jnp.float32)
+        gain = jnp.concatenate(
+            [mgain_buf[pl.ds(behind(step) * per_cols + i, 1), :] for i in range(per_cols)], axis=1
+        )
+        weighted = (mixed_float * gain).astype(jnp.bfloat16)
+        gate_copy(step).wait()
+        gate_acc[...] += jnp.dot(weighted, gate_w[step], preferred_element_type=jnp.float32)
+        up_copy(step).wait()
+        up_acc[...] += jnp.dot(weighted, up_w[step], preferred_element_type=jnp.float32)
+        return squares_sum + jnp.sum(mixed_float * mixed_float, axis=1, keepdims=True)
+
+    def mixer_arrived(step, squares_sum):
+        pltpu.make_async_remote_copy(
+            src_ref=mixed_all.at[0],
+            dst_ref=mixed_all.at[step],
+            send_sem=mixed_ssem.at[step],
+            recv_sem=mixed_rsem.at[step],
+            device_id=coords(ahead(step)),
+            device_id_type=MESH,
+        ).wait_recv()
+        return mixer_step(step, squares_sum)
+
+    squares_sum = mixer_step(0, jnp.zeros((rows, 1), jnp.float32))
+    squares_sum = lax.fori_loop(1, group, mixer_arrived, squares_sum)
+    mixer_scale = lax.rsqrt(squares_sum / width + epsilon)
+    hidden_buf[...] = (silu(mixer_scale * gate_acc[...]) * (mixer_scale * up_acc[...])).astype(jnp.bfloat16)
+
+    def down_part(step):
+        down_copy(step).wait()
+        return jnp.dot(hidden_buf[...], down_w[step], preferred_element_type=jnp.float32)
+
+    def red_send(step):
+        return pltpu.make_async_remote_copy(
+            src_ref=down_send.at[step],
+            dst_ref=down_recv.at[step],
+            send_sem=red_ssem.at[step],
+            recv_sem=red_rsem.at[step],
+            device_id=coords(ahead(step)),
+            device_id_type=MESH,
+        )
+
+    @pl.loop(1, group)
+    def _(step):
+        down_send[step] = down_part(step).astype(jnp.bfloat16)
+        red_send(step).start()
+
+    final = mixed.astype(jnp.float32) + down_part(0)
+    for step in range(1, group):
+        red_send(step).wait_recv()
+        final = final + down_recv[step].astype(jnp.float32)
+    result[...] = final.astype(jnp.bfloat16)
+    state_store.wait()
+    for send in tok_sends + proj_sends + gated_sends + mixed_sends:
+        send.wait_send()
+    for step in range(1, group):
+        red_send(step).wait_send()
+
+
+def local(
+    kv_count,
+    tp_count,
+    tokens,
+    rec_state,
+    norm_gain,
+    w_query,
+    w_forget,
+    w_input,
+    w_outgate,
+    lower_bound,
+    head_gain,
+    w_heads_out,
+    mixer_gain,
+    w_gate,
+    w_up,
+    w_down,
+):
+    group = kv_count * tp_count
+    rows, cols = tokens.shape
+    head_count = rec_state.shape[1]
+    hidden = w_gate.shape[1]
+    model_width = norm_gain.shape[0]
+    head_width = head_count * HEAD_DIM
+    fits = (
+        rec_state.shape[0] == 1
+        and HEAD_DIM == LANES
+        and head_count % 8 == 0
+        and cols % LANES == 0
+        and hidden % LANES == 0
+        and w_down.shape[0] == hidden
+    )
+    if not fits:
+        return local_plain(
+            tokens, rec_state, norm_gain, w_query, w_forget, w_input, w_outgate, lower_bound,
+            head_gain, w_heads_out, mixer_gain, w_gate, w_up, w_down,
+        )
+    f32, bf16 = jnp.float32, jnp.bfloat16
+    dma = pltpu.SemaphoreType.DMA
+    vmem = pltpu.VMEM
+    scratch = [
+        vmem((tp_count, rows, cols), bf16),
+        vmem(rec_state.shape[1:], f32),
+        vmem(rec_state.shape[1:], f32),
+        vmem((model_width // LANES, LANES), f32),
+        vmem((head_count, LANES), f32),
+        vmem((head_count, LANES), f32),
+        vmem((model_width // LANES, LANES), f32),
+        vmem((4,) + w_query.shape, bf16),
+        vmem(w_heads_out.shape, bf16),
+        vmem((group, cols, hidden), bf16),
+        vmem((group, cols, hidden), bf16),
+        vmem((group, hidden, cols), bf16),
+        vmem((kv_count, 5, head_count, LANES), f32),
+        vmem((kv_count, 5, head_count, LANES), f32),
+        vmem((head_count, LANES), f32),
+        vmem((group, head_count, LANES), bf16),
+        vmem((kv_count, tp_count, head_count, LANES), f32),
+        vmem((group, rows, cols), bf16),
+        vmem((rows, hidden), f32),
+        vmem((rows, hidden), f32),
+        vmem((rows, hidden), bf16),
+        vmem((group, rows, cols), bf16),
+        vmem((group, rows, cols), bf16),
+        dma((7,)),
+        dma((4,)),
+        dma,
+        dma((group,)),
+        dma((group,)),
+        dma((group,)),
+        dma((tp_count,)),
+        dma((tp_count,)),
+        dma((kv_count,)),
+        dma((kv_count,)),
+        dma((group,)),
+        dma((group,)),
+        dma((group,)),
+        dma((group,)),
+        dma((group,)),
+        dma((group,)),
+    ]
+    return pl.pallas_call(
+        functools.partial(layer_kernel, kv_count, tp_count),
+        out_shape=(
+            jax.ShapeDtypeStruct(tokens.shape, bf16),
+            jax.ShapeDtypeStruct(rec_state.shape, f32),
+        ),
+        in_specs=[pl.BlockSpec(memory_space=pl.ANY)] * 14,
+        out_specs=(
+            pl.BlockSpec(memory_space=pltpu.VMEM),
+            pl.BlockSpec(memory_space=pl.ANY),
+        ),
+        scratch_shapes=scratch,
+        compiler_params=pltpu.CompilerParams(
+            collective_id=0, has_side_effects=True, vmem_limit_bytes=60 * 1024 * 1024
+        ),
+    )(
+        tokens,
+        rec_state,
+        norm_gain.reshape(-1, LANES),
+        w_query,
+        w_forget,
+        w_input,
+        w_outgate,
+        lower_bound.reshape(-1, LANES),
+        head_gain.reshape(-1, LANES),
+        w_heads_out,
+        mixer_gain.reshape(-1, LANES),
+        w_gate,
+        w_up,
+        w_down,
+    )
+
+
 def solution(mesh):
     placed = (
         P("dp", ("kv", "tp")),
@@ -120,7 +553,7 @@
         P(("kv", "tp"), None),
     )
     return jax.shard_map(
-        local,
+        functools.partial(local, mesh.shape["kv"], mesh.shape["tp"]),
         mesh=mesh,
         in_specs=placed,
         out_specs=(P("dp", ("kv", "tp")), P(("dp", "kv"), "tp", None, None)),

time: 141 us -> 33.2 us (0.24)
  blocking collectives: 62.7 us -> 0 us
  waiting for transfers between devices: 32.8 us -> 0 us
  Pallas kernels: 0 us -> 29.2 us
  matrix products: 20.4 us -> 0 us
  between operations: 14.9 us -> 0.64 us
  other arithmetic: 4.46 us -> 0 us
  local copies, waits for them, and re-layouts: 5.37 us -> 3.14 us
    all_gather x3 -> x0, blocking collectives: 42.9 us -> none  [the longest x1 16.1 us: local(): lax.all_gather(tokens, ('kv', 'tp'), axis=1, tiled=True).astype(jnp.float32)]
    unnamed x2 -> x0, waiting for transfers between devices: 32.8 us -> none
    pallas_call x0 -> x1, Pallas kernels: none -> 29.2 us  [local(): pl.pallas_call(functools.partial(layer_kernel, kv_count, tp_count), out_s...]
    dot_general x7 -> x0, matrix products: 20.4 us -> none  [the longest x1 11 us: channel_mixer(): return jnp.dot(hidden, w_down, preferred_element_type=jnp.float32)]
    unnamed x2 -> x0, blocking collectives: 19.8 us -> none
    reduce_sum x4 -> x0, other arithmetic: 1.66 us -> none  [the longest x1 1.25 us: local(): head_out = jnp.sum(query_act[:, :, :, None] * new_state, axis=2)]
    mul x3 -> x0, other arithmetic: 1.52 us -> none  [the longest x1 1.5 us: local(): gate_pre = row_scale * projected[:, 3]]
    dynamic_slice x2 -> x0, local copies, waits for them, and re-layouts: 1.43 us -> none  [the longest x1 0.84 us: local(): lax.dynamic_slice_in_dim(norm_gain, kv_index * col_block, col_block, 0)]
  transfers between devices with their start and end apart: 1 -> 0, of which waited for: 1 -> 0; matrix products, arithmetic and copies ran while one was open for 1% -> 0% of each run, Pallas kernels for 0% -> 0%
where the time goes in v1:
time: 33.2 us; the launch traced here: 33 us
  Pallas kernels  29.2 us (88%)
  local copies, waits for them, and re-layouts  3.14 us (9%)
  between operations  0.64 us (2%)
    pallas_call x1, Pallas kernels, local(): pl.pallas_call(functools.partial(layer_kernel, kv_count, tp_count), out_s...  29.2 us
    unnamed x2, local copies, waits for them, and re-layouts  3.14 us

profile of v1, /device:TPU:0, one launch (start us, length us, event | category | flops | bytes accessed | tf_op | source)
XLA Modules:
  0.0 33.0 jit_solution(17892687649322338711)
XLA Ops:
  0.6 29.2 %shard_map.149 = (bf16[4,512]{1,0:T(4,128)(2,1)}, f32[1,8,128,128]{3,2,1,0:T(8,128)}) custom-call(bf16[4,512]{1,0:T(4,128)(2,1)} %tokens.1, f32[1,8,128,128]{3,2,1,0:T(8,128)} %rec_state.1, f32[32,128]{1,0:T(8,128)} %bitcast.4, bf16[1024,1024]{1,0:T(8,128)(2,1)} %w_query.1, bf16[1024,1024]{1,0:T(8,128)(2,1)} %w_forget.1, bf16[1024,1024]{1,0:T(8,128)(2,1)} %w_input.1, ...), custom_call_target="tpu_custom_call" | custom-call | tf_op jit(solution)/shard_map/pallas_call | solution.py:505
  29.9 1.3 %copy.18 = bf16[4,512]{1,0:T(4,128)(2,1)} copy(bf16[4,512]{1,0:T(4,128)(2,1)} %get-tuple-element.4) | data formatting | bytes 8192
  31.1 1.9 %copy.19 = f32[1,8,128,128]{3,2,1,0:T(8,128)} copy(f32[1,8,128,128]{3,2,1,0:T(8,128)} %get-tuple-element.5) | data formatting | bytes 1048576

commit v2 on v1

--- a/solution.py
+++ b/solution.py
@@ -135,7 +135,6 @@
     new_state,
     tok_all,
     state_in,
-    state_out,
     ngain_buf,
     lower_buf,
     hgain_buf,
@@ -145,8 +144,12 @@
     gate_w,
     up_w,
     down_w,
+    proj_acc,
+    proj_float,
     proj_send,
     proj_recv,
+    square_send,
+    square_recv,
     head_rows,
     gated_all,
     gated_float,
@@ -164,6 +167,8 @@
     down_sem,
     tok_ssem,
     tok_rsem,
+    square_ssem,
+    square_rsem,
     proj_ssem,
     proj_rsem,
     gated_ssem,
@@ -185,17 +190,18 @@
     def coords(index):
         return {"kv": lax.div(index, tp_count), "tp": lax.rem(index, tp_count)}
 
-    def ahead(step):
-        return lax.rem(me + step, group)
-
-    def behind(step):
-        return lax.rem(me + group - step, group)
+    def peer(step):
+        other, bit = 0, 1
+        while bit < group:
+            other = other + lax.rem((me // bit) + (step // bit), 2) * bit
+            bit = 2 * bit
+        return other
 
     def rows_of(step):
-        return pl.ds(pl.multiple_of(behind(step) * cols, LANES), cols)
+        return pl.ds(pl.multiple_of(peer(step) * cols, LANES), cols)
 
     def cols_of(step):
-        return pl.ds(pl.multiple_of(ahead(step) * cols, LANES), cols)
+        return pl.ds(pl.multiple_of(peer(step) * cols, LANES), cols)
 
     tok_copy = pltpu.make_async_copy(tokens, tok_all.at[tp], small_sem.at[0])
     small_copies = [
@@ -205,10 +211,14 @@
         pltpu.make_async_copy(mixer_gain, mgain_buf, small_sem.at[4]),
     ]
     state_copy = pltpu.make_async_copy(rec_state.at[0], state_in, small_sem.at[5])
-    proj_copies = [
-        pltpu.make_async_copy(weight, proj_w.at[i], proj_sem.at[i])
-        for i, weight in enumerate((w_query, w_forget, w_input, w_outgate))
-    ]
+
+    def proj_copy(weight, step, which):
+        source = lax.rem(tp + tp_count - step, tp_count)
+        from_rows = pl.ds(pl.multiple_of(source * cols, LANES), cols)
+        return pltpu.make_async_copy(
+            weight.at[from_rows, :], proj_w.at[step, which], proj_sem.at[step, which]
+        )
+
     heads_copy = pltpu.make_async_copy(w_heads_out, heads_w, heads_sem)
 
     def gate_copy(step):
@@ -223,22 +233,41 @@
     tok_copy.start()
     for copy in small_copies:
         copy.start()
-    for copy in proj_copies:
-        copy.start()
+    for step in range(tp_count):
+        for which, weight in enumerate((w_query, w_forget, w_input, w_outgate)):
+            proj_copy(weight, step, which).start()
     state_copy.start()
     heads_copy.start()
 
     barrier = pltpu.get_barrier_semaphore()
     for step in range(1, group):
-        pl.semaphore_signal(barrier, inc=1, device_id=coords(ahead(step)), device_id_type=MESH)
+        pl.semaphore_signal(barrier, inc=1, device_id=coords(peer(step)), device_id_type=MESH)
     for step in range(group):
         gate_copy(step).start()
         up_copy(step).start()
-    for step in range(group):
+    for step in range(group - 1, -1, -1):
         down_copy(step).start()
+    per_cols = cols // LANES
+
+    def proj_part(step, which):
+        source = lax.rem(tp + tp_count - step, tp_count)
+        first = (kv * tp_count + source) * per_cols
+        gain_row = jnp.concatenate(
+            [ngain_buf[pl.ds(first + i, 1), :] for i in range(per_cols)], axis=1
+        )
+        scaled = (tok_all[source].astype(jnp.float32) * gain_row).astype(jnp.bfloat16)
+        proj_copy(w_query, step, which).wait()
+        return jnp.dot(scaled, proj_w[step, which], preferred_element_type=jnp.float32)
+
+    tok_copy.wait()
+    for copy in small_copies:
+        copy.wait()
+
+    @pl.loop(0, 4)
+    def _(which):
+        proj_acc[which] = proj_part(0, which)
+
     pl.semaphore_wait(barrier, group - 1)
-
-    tok_copy.wait()
     tok_sends = []
     for step in range(1, tp_count):
         send = pltpu.make_async_remote_copy(
@@ -251,8 +280,6 @@
         )
         send.start()
         tok_sends.append(send)
-    for copy in small_copies:
-        copy.wait()
     for step in range(1, tp_count):
         source = lax.rem(tp + tp_count - step, tp_count)
         pltpu.make_async_remote_copy(
@@ -264,43 +291,59 @@
             device_id_type=MESH,
         ).wait_recv()
 
-    tok_float = jnp.concatenate([tok_all[i].astype(jnp.float32) for i in range(tp_count)], axis=1)
-    squares = jnp.sum(tok_float * tok_float, axis=1, keepdims=True)
-    per_block = proj_rows // LANES
-    gain_row = jnp.concatenate(
-        [ngain_buf[pl.ds(kv * per_block + i, 1), :] for i in range(per_block)], axis=1
-    )
-    scaled = (tok_float * gain_row).astype(jnp.bfloat16)
-    square_rows = jnp.broadcast_to(squares, (rows, LANES))
-    for h in range(head_count):
-        proj_send[:, 4, h, :] = square_rows
+    squares = jnp.zeros((rows, 1), jnp.float32)
+    for i in range(tp_count):
+        block = tok_all[i].astype(jnp.float32)
+        squares = squares + jnp.sum(block * block, axis=1, keepdims=True)
+    square_send[...] = jnp.broadcast_to(squares, (rows, LANES))
+    square_sends = []
+    for step in range(kv_count - 1, 0, -1):
+        send = pltpu.make_async_remote_copy(
+            src_ref=square_send,
+            dst_ref=square_recv.at[step],
+            send_sem=square_ssem.at[step],
+            recv_sem=square_rsem.at[step],
+            device_id=coords(peer(step * tp_count)),
+            device_id_type=MESH,
+        )
+        send.start()
+        square_sends.append(send)
 
     @pl.loop(0, 4)
     def _(which):
-        pltpu.make_async_copy(w_query, proj_w.at[which], proj_sem.at[which]).wait()
-        part = jnp.dot(scaled, proj_w[which], preferred_element_type=jnp.float32)
+        part = proj_acc[which]
+        for step in range(1, tp_count):
+            part = part + proj_part(step, which)
         for h in range(head_count):
-            proj_send[:, which, h, :] = part[:, h * LANES : (h + 1) * LANES]
-
+            proj_float[:, which, h, :] = part[:, h * LANES : (h + 1) * LANES]
+
+    proj_send[...] = proj_float[...].astype(jnp.bfloat16)
     proj_sends = []
-    for step in range(1, kv_count):
-        target = lax.rem(kv + step, kv_count)
+    for step in range(kv_count - 1, 0, -1):
+        target = peer(step * tp_count)
         send = pltpu.make_async_remote_copy(
-            src_ref=proj_send.at[target],
+            src_ref=proj_send.at[lax.div(target, tp_count)],
             dst_ref=proj_recv.at[step],
             send_sem=proj_ssem.at[step],
             recv_sem=proj_rsem.at[step],
-            device_id={"kv": target},
+            device_id=coords(target),
             device_id_type=MESH,
         )
         send.start()
         proj_sends.append(send)
-    total = proj_send[kv]
+    total = proj_float[kv]
+    square_recv[0] = square_send[...]
     state_copy.wait()
     for step in range(1, kv_count):
-        proj_sends[step - 1].wait_recv()
-        total = total + proj_recv[step]
-    row_scale = lax.rsqrt(total[4] / width + epsilon)
+        square_sends[kv_count - 1 - step].wait_recv()
+    every_square = square_recv[0]
+    for step in range(1, kv_count):
+        every_square = every_square + square_recv[step]
+    square_recv[0] = every_square
+    row_scale = lax.rsqrt(square_recv[0, pl.ds(kv, 1), :] / width + epsilon)
+    for step in range(1, kv_count):
+        proj_sends[kv_count - 1 - step].wait_recv()
+        total = total + proj_recv[step].astype(jnp.float32)
     query_act = silu(row_scale * total[0])
     lower = lower_buf[...]
     forget = lower + (1.0 - lower) / (1.0 + jnp.exp(-(row_scale * total[1])))
@@ -312,31 +355,29 @@
     query_t = query_act.T
     for h in range(head_count):
         fresh = forget_t[:, h : h + 1] * state_in[h] + key_t[:, h : h + 1] * value_in[h : h + 1, :]
-        state_out[h] = fresh
+        new_state[0, h] = fresh
         head_rows[h : h + 1, :] = jnp.sum(query_t[:, h : h + 1] * fresh, axis=0, keepdims=True)
     head_out = head_rows[...]
     head_out = head_out * lax.rsqrt(jnp.mean(head_out * head_out, axis=1, keepdims=True) + epsilon)
     gated_all[0] = (head_out * hgain_buf[...] * gate_act).astype(jnp.bfloat16)
 
     gated_sends = []
-    for step in range(1, group):
+    for step in range(group - 1, 0, -1):
         send = pltpu.make_async_remote_copy(
             src_ref=gated_all.at[0],
             dst_ref=gated_all.at[step],
             send_sem=gated_ssem.at[step],
             recv_sem=gated_rsem.at[step],
-            device_id=coords(ahead(step)),
+            device_id=coords(peer(step)),
             device_id_type=MESH,
         )
         send.start()
         gated_sends.append(send)
-    state_store = pltpu.make_async_copy(state_out, new_state.at[0], small_sem.at[6])
-    state_store.start()
     gated_float[kv, tp] = gated_all[0].astype(jnp.float32)
     heads_copy.wait()
     for step in range(1, group):
-        gated_sends[step - 1].wait_recv()
-        source = behind(step)
+        gated_sends[group - 1 - step].wait_recv()
+        source = peer(step)
         gated_float[lax.div(source, tp_count), lax.rem(source, tp_count)] = gated_all[step].astype(jnp.float32)
     every_head = jnp.concatenate(
         [gated_float[:, t, h, :] for t in range(tp_count) for h in range(head_count)], axis=1
@@ -346,13 +387,13 @@
     mixed_all[0] = mixed
 
     mixed_sends = []
-    for step in range(1, group):
+    for step in range(group - 1, 0, -1):
         send = pltpu.make_async_remote_copy(
             src_ref=mixed_all.at[0],
             dst_ref=mixed_all.at[step],
             send_sem=mixed_ssem.at[step],
             recv_sem=mixed_rsem.at[step],
-            device_id=coords(ahead(step)),
+            device_id=coords(peer(step)),
             device_id_type=MESH,
         )
         send.start()
@@ -360,12 +401,11 @@
 
     gate_acc[...] = jnp.zeros_like(gate_acc)
     up_acc[...] = jnp.zeros_like(up_acc)
-    per_cols = cols // LANES
 
     def mixer_step(step, squares_sum):
         mixed_float = mixed_all[step].astype(jnp.float32)
         gain = jnp.concatenate(
-            [mgain_buf[pl.ds(behind(step) * per_cols + i, 1), :] for i in range(per_cols)], axis=1
+            [mgain_buf[pl.ds(peer(step) * per_cols + i, 1), :] for i in range(per_cols)], axis=1
         )
         weighted = (mixed_float * gain).astype(jnp.bfloat16)
         gate_copy(step).wait()
@@ -380,7 +420,7 @@
             dst_ref=mixed_all.at[step],
             send_sem=mixed_ssem.at[step],
             recv_sem=mixed_rsem.at[step],
-            device_id=coords(ahead(step)),
+            device_id=coords(peer(step)),
             device_id_type=MESH,
         ).wait_recv()
         return mixer_step(step, squares_sum)
@@ -400,12 +440,13 @@
             dst_ref=down_recv.at[step],
             send_sem=red_ssem.at[step],
             recv_sem=red_rsem.at[step],
-            device_id=coords(ahead(step)),
+            device_id=coords(peer(step)),
             device_id_type=MESH,
         )
 
     @pl.loop(1, group)
-    def _(step):
+    def _(turn):
+        step = group - turn
         down_send[step] = down_part(step).astype(jnp.bfloat16)
         red_send(step).start()
 
@@ -414,11 +455,25 @@
         red_send(step).wait_recv()
         final = final + down_recv[step].astype(jnp.float32)
     result[...] = final.astype(jnp.bfloat16)
-    state_store.wait()
-    for send in tok_sends + proj_sends + gated_sends + mixed_sends:
+    for send in tok_sends + square_sends + proj_sends + gated_sends + mixed_sends:
         send.wait_send()
     for step in range(1, group):
         red_send(step).wait_send()
+
+
+def store_kernel(held, state, result, new_state, sems):
+    copies = [
+        pltpu.make_async_copy(held, result, sems.at[0]),
+        pltpu.make_async_copy(state, new_state, sems.at[1]),
+    ]
+    for copy in copies:
+        copy.start()
+    for copy in copies:
+        copy.wait()
+
+
+def in_hbm(*arrays):
+    return [pltpu.with_memory_space_constraint(array, pltpu.HBM) for array in arrays]
 
 
 def local(
@@ -447,6 +502,8 @@
     head_width = head_count * HEAD_DIM
     fits = (
         rec_state.shape[0] == 1
+        and group & (group - 1) == 0
+        and tp_count & (tp_count - 1) == 0
         and HEAD_DIM == LANES
         and head_count % 8 == 0
         and cols % LANES == 0
@@ -464,18 +521,21 @@
     scratch = [
         vmem((tp_count, rows, cols), bf16),
         vmem(rec_state.shape[1:], f32),
-        vmem(rec_state.shape[1:], f32),
         vmem((model_width // LANES, LANES), f32),
         vmem((head_count, LANES), f32),
         vmem((head_count, LANES), f32),
         vmem((model_width // LANES, LANES), f32),
-        vmem((4,) + w_query.shape, bf16),
+        vmem((tp_count, 4, cols, w_query.shape[1]), bf16),
         vmem(w_heads_out.shape, bf16),
         vmem((group, cols, hidden), bf16),
         vmem((group, cols, hidden), bf16),
         vmem((group, hidden, cols), bf16),
-        vmem((kv_count, 5, head_count, LANES), f32),
-        vmem((kv_count, 5, head_count, LANES), f32),
+        vmem((4, rows, w_query.shape[1]), f32),
+        vmem((kv_count, 4, head_count, LANES), f32),
+        vmem((kv_count, 4, head_count, LANES), bf16),
+        vmem((kv_count, 4, head_count, LANES), bf16),
+        vmem((rows, LANES), f32),
+        vmem((kv_count, rows, LANES), f32),
         vmem((head_count, LANES), f32),
         vmem((group, head_count, LANES), bf16),
         vmem((kv_count, tp_count, head_count, LANES), f32),
@@ -485,8 +545,8 @@
         vmem((rows, hidden), bf16),
         vmem((group, rows, cols), bf16),
         vmem((group, rows, cols), bf16),
-        dma((7,)),
-        dma((4,)),
+        dma((6,)),
+        dma((tp_count, 4)),
         dma,
         dma((group,)),
         dma((group,)),
@@ -495,6 +555,8 @@
         dma((tp_count,)),
         dma((kv_count,)),
         dma((kv_count,)),
+        dma((kv_count,)),
+        dma((kv_count,)),
         dma((group,)),
         dma((group,)),
         dma((group,)),
@@ -502,22 +564,23 @@
         dma((group,)),
         dma((group,)),
     ]
-    return pl.pallas_call(
+    held, state = pl.pallas_call(
         functools.partial(layer_kernel, kv_count, tp_count),
         out_shape=(
-            jax.ShapeDtypeStruct(tokens.shape, bf16),
-            jax.ShapeDtypeStruct(rec_state.shape, f32),
+            pltpu.VMEM(tokens.shape, bf16),
+            pltpu.VMEM(rec_state.shape, f32),
         ),
-        in_specs=[pl.BlockSpec(memory_space=pl.ANY)] * 14,
+        in_specs=[pl.BlockSpec(memory_space=pltpu.HBM)] * 14,
         out_specs=(
             pl.BlockSpec(memory_space=pltpu.VMEM),
-            pl.BlockSpec(memory_space=pl.ANY),
+            pl.BlockSpec(memory_space=pltpu.VMEM),
         ),
         scratch_shapes=scratch,
         compiler_params=pltpu.CompilerParams(
-            collective_id=0, has_side_effects=True, vmem_limit_bytes=60 * 1024 * 1024
+            collective_id=0, has_side_effects=True, vmem_limit_bytes=52 * 1024 * 1024
         ),
     )(
+        *in_hbm(
         tokens,
         rec_state,
         norm_gain.reshape(-1, LANES),
@@ -532,6 +595,20 @@
         w_gate,
         w_up,
         w_down,
+        )
+    )
+    return pl.pallas_call(
+        store_kernel,
+        out_shape=(
+            jax.ShapeDtypeStruct(tokens.shape, bf16),
+            jax.ShapeDtypeStruct(rec_state.shape, f32),
+        ),
+        in_specs=[pl.BlockSpec(memory_space=pl.ANY)] * 2,
+        out_specs=(pl.BlockSpec(memory_space=pl.ANY), pl.BlockSpec(memory_space=pl.ANY)),
+        scratch_shapes=[dma((2,))],
+    )(
+        pltpu.with_memory_space_constraint(held, pltpu.VMEM),
+        pltpu.with_memory_space_constraint(state, pltpu.VMEM),
     )
 
 

time: 33.2 us -> 31 us (0.934)
  local copies, waits for them, and re-layouts: 3.14 us -> 0 us
  Pallas kernels: 29.2 us -> 30.2 us
    unnamed x2 -> x0, local copies, waits for them, and re-layouts: 3.14 us -> none
    pallas_call x0 -> x1, Pallas kernels: none -> 0.82 us  [local(): pl.pallas_call(store_kernel, out_shape=(jax.ShapeDtypeStruct(tokens.shape...]
where the time goes in v2:
time: 31 us; the launch traced here: 30.9 us
  Pallas kernels  30.2 us (97%)
  between operations  0.64 us (2%)
    pallas_call x1, Pallas kernels, local(): pl.pallas_call(functools.partial(layer_kernel, kv_count, tp_count), out_s...  29.4 us
    pallas_call x1, Pallas kernels, local(): pl.pallas_call(store_kernel, out_shape=(jax.ShapeDtypeStruct(tokens.shape...  0.82 us

profile of v2, /device:TPU:0, one launch (start us, length us, event | category | flops | bytes accessed | tf_op | source)
XLA Modules:
  0.0 30.9 jit_solution(8360999345152046265)
XLA Ops:
  0.6 29.4 %shard_map.149 = (bf16[4,512]{1,0:T(4,128)(2,1)S(1)}, f32[1,8,128,128]{3,2,1,0:T(8,128)S(1)}) custom-call(bf16[4,512]{1,0:T(4,128)(2,1)} %tokens.1, f32[1,8,128,128]{3,2,1,0:T(8,128)} %rec_state.1, f32[32,128]{1,0:T(8,128)} %bitcast.4, bf16[1024,1024]{1,0:T(8,128)(2,1)} %w_query.1, bf16[1024,1024]{1,0:T(8,128)(2,1)} %w_forget.1, bf16[1024,1024]{1,0:T(8,128)(2,1)} %w_input.1, ...), custom_call_target="tpu_custom_call" | custom-call | tf_op jit(solution)/shard_map/pallas_call | solution.py:567
  30.0 0.8 %shard_map.150 = (bf16[4,512]{1,0:T(4,128)(2,1)}, f32[1,8,128,128]{3,2,1,0:T(8,128)}) custom-call(bf16[4,512]{1,0:T(4,128)(2,1)S(1)} %get-tuple-element.4.held, f32[1,8,128,128]{3,2,1,0:T(8,128)S(1)} %get-tuple-element.5.state), custom_call_target="tpu_custom_call" | custom-call | tf_op jit(solution)/shard_map/pallas_call | solution.py:600
